TPU v7x, 32 devices: a whole 2x2x4 slice. The times are simulated.
32 devices in a mesh: ep: 8 (over z, x), tp: 4 (over y, core).
Axes of the slice: x: 2, y: 2, z: 4, core: 2. Of those that a mesh axis runs over, the one named last changes fastest.
Arguments:
- hidden_in: bfloat16 [128, 2048], P(None, 'ep'), may hold values from -24 to 24
- attn_gain: float32 [2048], replicated, may hold values from 0.1 to 1.9
- forget_weight: bfloat16 [2048, 16], replicated, may hold values from -0.125 to 0.125
- forget_bias: float32 [16], replicated, may hold values from -1 to 2
- query_weight: bfloat16 [2048, 2048], P('ep', 'tp'), may hold values from -0.125 to 0.125
- key_weight: bfloat16 [2048, 1024], P('ep', 'tp'), may hold values from -0.125 to 0.125
- value_weight: bfloat16 [2048, 1024], P('ep', 'tp'), may hold values from -0.125 to 0.125
- query_gain: float32 [128], replicated, may hold values from 0.1 to 1.9
- key_gain: float32 [128], replicated, may hold values from 0.1 to 1.9
- cache_keys: bfloat16 [128, 8, 1024, 128], P('ep', 'tp'), may hold values from -160 to 160
- cache_values: bfloat16 [128, 8, 1024, 128], P('ep', 'tp'), may hold values from -6 to 6
- cache_gates: float32 [128, 16, 1024], P('ep', 'tp'), may hold values from -256 to 0, as said below
- lengths: int32 [128], P('ep'), may hold values from 128 to 1024, as said below
- output_weight: bfloat16 [2048, 2048], P('tp', 'ep'), may hold values from -0.125 to 0.125
- ffn_gain: float32 [2048], replicated, may hold values from 0.1 to 1.9
- route_group: int32 [128], replicated, may hold values from 0 to 3, as said below
- route_expert: int32 [128, 2], replicated, may hold values from 0 to 3, as said below
- route_weight: float32 [128, 2], replicated, may hold values from 0.1 to 0.6
- expert_gate: bfloat16 [16, 2048, 1024], P('ep', None, 'tp'), may hold values from -0.125 to 0.125
- expert_up: bfloat16 [16, 2048, 1024], P('ep', None, 'tp'), may hold values from -0.125 to 0.125
- expert_down: bfloat16 [16, 1024, 2048], P('ep', 'tp'), may hold values from -0.1875 to 0.1875
- mix_vector: bfloat16 [2048], replicated, may hold values from -0.125 to 0.125
- dense_gate: bfloat16 [2048, 4096], P('ep', 'tp'), may hold values from -0.125 to 0.125
- dense_up: bfloat16 [2048, 4096], P('ep', 'tp'), may hold values from -0.125 to 0.125
- dense_down: bfloat16 [4096, 2048], P('tp', 'ep'), may hold values from -0.09375 to 0.09375
Outputs:
- mixed: bfloat16 [128, 2048], P(None, 'ep')
- fresh_keys: bfloat16 [128, 1024], P('ep', 'tp')
- fresh_values: bfloat16 [128, 1024], P('ep', 'tp')
Inputs may be any that keep to these rules, and one draw needn't show every extreme that they name: `cache_gates`: never rising along positions. `lengths`: some device holds a sequence of length 1024 in every draw. `route_group`: no expert is chosen by more than 24 tokens of the batch, and some expert by exactly 24. `route_expert`: a token's 2 experts differ; the loads of the experts of one group differ by at most two.
All inputs are finite; a program needn't handle non-finite values.
Results may differ from a plain program's by a relative error of at most 0.008.
Values may be sent and summed in bfloat16 or wider, within the bound.
A program may use at most 64 MiB of HBM per device.

v0:
```python
import jax
import jax.numpy as jnp
from jax import lax
from jax.sharding import PartitionSpec as P

D = 2048
HEAD_DIM = 128
GROUP_EXPERTS = 4
TOPK = 2
CAPACITY = 24
EPS = 1e-06


def head_norm(projected, gain_vec):
    return (
        projected
        * lax.rsqrt(jnp.mean(projected * projected, axis=-1, keepdims=True) + EPS)
        * gain_vec
    )


def slot_targets(route_group, route_expert, expert_count):
    chosen = (route_group[:, None] * GROUP_EXPERTS + route_expert).reshape(-1)
    onehot = (chosen[:, None] == jnp.arange(expert_count, dtype=jnp.int32)[None, :]).astype(
        jnp.int32
    )
    before = jnp.cumsum(onehot, axis=0) - onehot
    return chosen * CAPACITY + jnp.sum(before * onehot, axis=1)


def on_device(
    hidden_in,
    attn_gain,
    forget_weight,
    forget_bias,
    query_weight,
    key_weight,
    value_weight,
    query_gain,
    key_gain,
    cache_keys,
    cache_values,
    cache_gates,
    lengths,
    output_weight,
    ffn_gain,
    route_group,
    route_expert,
    route_weight,
    expert_gate,
    expert_up,
    expert_down,
    mix_vector,
    dense_gate,
    dense_up,
    dense_down,
):
    seq_count, width_block = hidden_in.shape
    own_count = cache_keys.shape[0]
    ep_index = lax.axis_index("ep")
    tp_index = lax.axis_index("tp")
    ep_count = lax.axis_size("ep")
    col_start = ep_index * width_block
    row_start = ep_index * own_count
    stream = hidden_in.astype(jnp.float32)
    normed_in = (stream * lax.dynamic_slice_in_dim(attn_gain, col_start, width_block)).astype(
        jnp.bfloat16
    )
    forget_rows = lax.dynamic_slice_in_dim(forget_weight, col_start, width_block, 0)
    squares, forget_dot = lax.psum(
        (
            jnp.sum(stream * stream, axis=1),
            jnp.dot(normed_in, forget_rows, preferred_element_type=jnp.float32),
        ),
        "ep",
    )
    inv_rms = lax.rsqrt(squares / D + EPS)
    query_cols = query_weight.shape[1]
    key_cols = key_weight.shape[1]
    selected = normed_in
    head_sums = lax.psum_scatter(
        jnp.concatenate(
            [
                jnp.dot(selected, query_weight, preferred_element_type=jnp.float32),
                jnp.dot(selected, key_weight, preferred_element_type=jnp.float32),
                jnp.dot(selected, value_weight, preferred_element_type=jnp.float32),
            ],
            axis=1,
        ),
        "ep",
        scatter_dimension=0,
        tiled=True,
    )
    heads_here = query_cols // HEAD_DIM
    kv_here = key_cols // HEAD_DIM
    group_size = heads_here // kv_here
    own_scale = lax.dynamic_slice_in_dim(inv_rms, row_start, own_count)
    query_rows = head_norm(
        head_sums[:, :query_cols].reshape(own_count, heads_here, HEAD_DIM), query_gain
    ).astype(jnp.bfloat16)
    fresh_key = head_norm(
        head_sums[:, query_cols : query_cols + key_cols].reshape(own_count, kv_here, HEAD_DIM),
        key_gain,
    ).astype(jnp.bfloat16)
    fresh_value = (head_sums[:, query_cols + key_cols :] * own_scale[:, None]).astype(jnp.bfloat16)
    gate_logit = lax.dynamic_slice(
        forget_dot, (row_start, tp_index * heads_here), (own_count, heads_here)
    )
    bias_here = lax.dynamic_slice_in_dim(forget_bias, tp_index * heads_here, heads_here)
    log_forget = jax.nn.log_sigmoid(gate_logit * own_scale[:, None] + bias_here)
    latest = jnp.take_along_axis(cache_gates, (lengths - 1)[:, None, None], axis=2)[:, :, 0]
    now_gate = (latest + log_forget).reshape(own_count, kv_here, group_size)
    grouped = query_rows.reshape(own_count, kv_here, group_size, HEAD_DIM)
    factor = HEAD_DIM ** (-0.5)
    scores = (
        jnp.einsum("skgd,skcd->skgc", grouped, cache_keys, preferred_element_type=jnp.float32)
        * factor
    )
    scores = scores + now_gate[..., None] - cache_gates.reshape(own_count, kv_here, group_size, -1)
    in_cache = (
        jnp.arange(cache_keys.shape[2], dtype=jnp.int32)[None, None, None, :]
        < lengths[:, None, None, None]
    )
    scores = jnp.where(in_cache, scores, -jnp.inf)
    self_score = (
        jnp.einsum("skgd,skd->skg", grouped, fresh_key, preferred_element_type=jnp.float32) * factor
    )
    ceiling = jnp.maximum(jnp.max(scores, axis=-1), self_score)
    weights = jnp.exp(scores - ceiling[..., None])
    self_weight = jnp.exp(self_score - ceiling)
    denominator = jnp.sum(weights, axis=-1) + self_weight
    mixed_heads = jnp.einsum(
        "skgc,skcd->skgd",
        weights.astype(jnp.bfloat16),
        cache_values,
        preferred_element_type=jnp.float32,
    )
    mixed_heads = mixed_heads + self_weight[..., None] * fresh_value.reshape(
        own_count, kv_here, 1, HEAD_DIM
    ).astype(jnp.float32)
    heads_out = (
        (mixed_heads / denominator[..., None]).reshape(own_count, query_cols).astype(jnp.bfloat16)
    )
    attn_part = jnp.dot(
        lax.all_gather(heads_out, "ep", axis=0, tiled=True),
        output_weight,
        preferred_element_type=jnp.float32,
    )
    attn_out = lax.psum(attn_part, "tp")
    middle = (stream + attn_out).astype(jnp.bfloat16).astype(jnp.float32)
    normed_mid = (middle * lax.dynamic_slice_in_dim(ffn_gain, col_start, width_block)).astype(
        jnp.bfloat16
    )
    mix_part = jnp.dot(
        normed_mid,
        lax.dynamic_slice_in_dim(mix_vector, col_start, width_block),
        preferred_element_type=jnp.float32,
    )
    squares_mid, mix_dot = lax.psum((jnp.sum(middle * middle, axis=1), mix_part), "ep")
    mid_scale = lax.rsqrt(squares_mid / D + EPS)
    mix_share = jax.nn.sigmoid(mid_scale * mix_dot)
    local_experts = expert_gate.shape[0]
    expert_count = local_experts * ep_count
    targets = slot_targets(route_group, route_expert, expert_count)
    slot_total = expert_count * CAPACITY
    slot_ids = jnp.arange(slot_total, dtype=jnp.int32)
    placed = jnp.any(
        targets.reshape(seq_count, TOPK)[None, :, :] == slot_ids[:, None, None], axis=2
    )
    outgoing = jnp.dot(placed.astype(jnp.bfloat16), normed_mid, preferred_element_type=jnp.float32)
    outgoing = outgoing.astype(jnp.bfloat16).reshape(ep_count, local_experts, CAPACITY, width_block)
    arrived = lax.all_to_all(outgoing, "ep", split_axis=0, concat_axis=3, tiled=True).reshape(
        local_experts, CAPACITY, -1
    )
    my_slots = lax.dynamic_slice_in_dim(
        placed, ep_index * local_experts * CAPACITY, local_experts * CAPACITY, 0
    )
    slot_scale = jnp.sum(jnp.where(my_slots, mid_scale[None, :], 0.0), axis=1).reshape(
        local_experts, CAPACITY, 1
    )
    gate_pre = (
        jnp.einsum("ecd,edf->ecf", arrived, expert_gate, preferred_element_type=jnp.float32)
        * slot_scale
    )
    up_pre = (
        jnp.einsum("ecd,edf->ecf", arrived, expert_up, preferred_element_type=jnp.float32)
        * slot_scale
    )
    expert_hidden = (jax.nn.silu(gate_pre) * up_pre).astype(jnp.bfloat16)
    expert_part = jnp.einsum(
        "ecf,efd->ecd", expert_hidden, expert_down, preferred_element_type=jnp.float32
    )
    returned = (
        lax.all_to_all(
            expert_part[None].astype(jnp.bfloat16), "ep", split_axis=3, concat_axis=0, tiled=True
        )
        .astype(jnp.float32)
        .reshape(slot_total, width_block)
    )
    picked = jnp.take(returned, targets, axis=0).reshape(seq_count, TOPK, width_block)
    routed = jnp.sum(picked * route_weight[:, :, None], axis=1)
    hidden_width = dense_gate.shape[1]
    selected = normed_mid
    both_sums = lax.psum_scatter(
        jnp.concatenate(
            [
                jnp.dot(selected, dense_gate, preferred_element_type=jnp.float32),
                jnp.dot(selected, dense_up, preferred_element_type=jnp.float32),
            ],
            axis=1,
        ),
        "ep",
        scatter_dimension=0,
        tiled=True,
    )
    gate_sum = both_sums[:, :hidden_width]
    up_sum = both_sums[:, hidden_width:]
    own_mid = lax.dynamic_slice_in_dim(mid_scale, row_start, own_count)
    dense_hidden = (jax.nn.silu(gate_sum * own_mid[:, None]) * (up_sum * own_mid[:, None])).astype(
        jnp.bfloat16
    )
    dense_part = jnp.dot(
        lax.all_gather(dense_hidden, "ep", axis=0, tiled=True),
        dense_down,
        preferred_element_type=jnp.float32,
    )
    ffn_total = lax.psum(
        (routed + mix_share[:, None] * dense_part).astype(jnp.bfloat16), "tp"
    ).astype(jnp.float32)
    mixed = (middle + ffn_total).astype(jnp.bfloat16)
    return (mixed, fresh_key.reshape(own_count, key_cols), fresh_value)


def solution(mesh):
    placed = (
        P(None, "ep"),
        P(),
        P(),
        P(),
        P("ep", "tp"),
        P("ep", "tp"),
        P("ep", "tp"),
        P(),
        P(),
        P("ep", "tp", None, None),
        P("ep", "tp", None, None),
        P("ep", "tp", None),
        P("ep"),
        P("tp", "ep"),
        P(),
        P(),
        P(),
        P(),
        P("ep", None, "tp"),
        P("ep", None, "tp"),
        P("ep", "tp", None),
        P(),
        P("ep", "tp"),
        P("ep", "tp"),
        P("tp", "ep"),
    )
    return jax.shard_map(
        on_device,
        mesh=mesh,
        in_specs=placed,
        out_specs=(P(None, "ep"), P("ep", "tp"), P("ep", "tp")),
        check_vma=False,
    )
```

profile of v0, /device:TPU:0, one launch (start us, length us, event | category | flops | bytes accessed | tf_op | source)
XLA Modules:
  0.0 295.3 jit_solution(9477003200772531910)
XLA Ops:
  8.2 1.2 fusion.40
  9.4 1.1 fusion.36
  10.5 1.1 fusion.38
  13.6 23.6 %all-reduce.1 = (f32[128,16]{0,1:T(8,128)S(1)}, f32[128]{0:T(128)S(1)}) all-reduce(f32[128,16]{0,1:T(8,128)S(1)} %fusion.34, f32[128]{0:T(128)S(1)} %fusion.15), channel_id=1, replica_groups=mesh['ep'=8,'tp'=4] {'ep'}, use_global_device_ids=true, to_apply=%region_2.0 | all-reduce | flops 2176 | bytes 17408 | tf_op jit(solution)/shard_map/psum | solution.py:70
  37.4 4.7 %copy.71 = f32[16,4,1024]{1,2,0:T(8,128)} copy(f32[16,4,1024]{2,1,0:T(4,128)S(1)} %copy-done.4) | data formatting | bytes 524288 | tf_op args[11]
  43.2 1.3 gather_fusion.1
  47.9 30.2 %reduce-scatter.3.cloned.1.call-done = f32[16,1024]{1,0:T(8,128)} async-done(((f32[128,1024]{1,0:T(8,128)}), f32[16,1024]{1,0:T(8,128)}) %reduce-scatter.3.cloned.1.call-update) | async-done | bytes 65552 | tf_op jit(solution)/shard_map/reduce_scatter | solution.py:81
  80.4 5.8 %fusion.64 = (f32[16,2,2]{2,1,0:T(2,128)S(1)}, f32[16,2,2,1024]{3,2,1,0:T(2,128)S(1)}) fusion(f32[16,2,2,1024]{3,2,1,0:T(2,128)S(1)} %reshape.201, f32[16,2,2]{2,1,0:T(2,128)S(1)} %copy.73, bf16[16,2,2,128]{3,2,1,0:T(2,128)(2,1)S(1)} %multiply_convert_fusion, bf16[16,2,1024,128]{3,2,1,0:T(8,128)(2,1)} %param.34, pred[16,1024]{1,0:T(8,128)(4,1)S(1)} %iota_compare_fusion.1), kind=kOutput, calls=%fused_computation.109 | convolution fusion | flops 17104832 | bytes 8946176 | tf_op jit(solution)/shard_map/skgd,skcd->skgc/dot_general | solution.py:116
  87.3 5.4 %fusion.9 = bf16[16,2,2,128]{3,2,1,0:T(2,128)(2,1)} fusion(bf16[16,2,1024,128]{3,2,1,0:T(8,128)(2,1)} %param.35, f32[16,2,2,1024]{3,2,1,0:T(2,128)S(1)} %get-tuple-element.22, f32[16,2,2]{2,1,0:T(2,128)S(1)} %multiply_maximum_fusion, f32[16,2,2]{2,1,0:T(2,128)S(1)} %get-tuple-element.13, f32[16,2,128]{2,1,0:T(2,128)S(1)} %reshape.207, ...), kind=kOutput, calls=%fused_computation.18 | convolution fusion | flops 16941056 | bytes 8684288 | tf_op jit(solution)/shard_map/skgc,skcd->skgd/dot_general | solution.py:132
  93.5 30.5 %all_gather.6 = bf16[128,512]{1,0:T(8,128)(2,1)S(1)} all-gather(bf16[16,512]{1,0:T(8,128)(2,1)S(1)} %convert_element_type.102), channel_id=1, replica_groups=mesh['ep'=8,'tp'=4] {'ep'}, dimensions={0}, use_global_device_ids=true | all-gather | bytes 147456 | tf_op jit(solution)/shard_map/all_gather | solution.py:145
  125.2 30.6 %all-reduce.5.cloned.1.call-done = f32[128,256]{1,0:T(8,128)} async-done(((f32[128,256]{1,0:T(8,128)}), f32[128,256]{1,0:T(8,128)}) %all-reduce.5.cloned.1.call-update) | async-done | bytes 131088 | tf_op jit(solution)/shard_map/psum | solution.py:149
  159.4 5.5 %all-to-all-start = ((bf16[8,2,24,256]{3,2,1,0:T(8,128)(2,1)}), bf16[8,2,24,256]{3,2,1,0:T(8,128)(2,1)S(1)}, u32[]{:S(2)}, u32[]{:S(2)}) async-start(bf16[8,2,24,256]{3,2,1,0:T(8,128)(2,1)} %bitcast.9), calls=%async_computation.1 | async-start | bytes 393216 | tf_op jit(solution)/shard_map/all_to_all | solution.py:172
  165.0 21.9 %all-reduce = (f32[128]{0:T(128)S(1)}, f32[128]{0:T(128)S(1)}) all-reduce(f32[128]{0:T(128)S(1)} %get-tuple-element.11, f32[128]{0:T(128)S(1)} %convolution_bitcast_fusion), channel_id=1, replica_groups=mesh['ep'=8,'tp'=4] {'ep'}, use_global_device_ids=true, to_apply=%region_14.15 | all-reduce | flops 256 | bytes 2048 | tf_op jit(solution)/shard_map/psum | solution.py:159
  187.9 1.9 convolution_multiply_fusion.3
  189.9 2.3 fusion
  193.0 2.0 reshape.232
  195.0 3.4 %all-to-all-start.1 = ((bf16[8,2,6144]{2,1,0:T(2,128)(2,1)}), bf16[8,2,6144]{2,1,0:T(2,128)(2,1)S(1)}, u32[]{:S(2)}, u32[]{:S(2)}) async-start(bf16[8,2,6144]{2,1,0:T(2,128)(2,1)} %reshape.232), calls=%async_computation.2 | async-start | bytes 393216 | tf_op jit(solution)/shard_map/all_to_all | solution.py:194
  201.0 5.2 %all-to-all-done.1 = bf16[8,2,6144]{2,1,0:T(2,128)(2,1)S(1)} async-done(((bf16[8,2,6144]{2,1,0:T(2,128)(2,1)}), bf16[8,2,6144]{2,1,0:T(2,128)(2,1)S(1)}, u32[]{:S(2)}, u32[]{:S(2)}) %all-to-all-start.1) | async-done | bytes 196640 | tf_op jit(solution)/shard_map/all_to_all | solution.py:194
  206.1 1.5 reshape.233
  208.2 1.2 gather_fusion
  210.5 13.5 %reduce-scatter.5.cloned.1.call-done = f32[16,2048]{1,0:T(8,128)} async-done(((f32[128,2048]{1,0:T(8,128)}), f32[16,2048]{1,0:T(8,128)}) %reduce-scatter.5.cloned.1.call-update) | async-done | bytes 131088 | tf_op jit(solution)/shard_map/reduce_scatter | solution.py:204
  225.0 30.9 %all_gather.7 = bf16[128,1024]{1,0:T(8,128)(2,1)S(1)} all-gather(bf16[16,1024]{1,0:T(8,128)(2,1)S(1)} %fusion.22), channel_id=1, replica_groups=mesh['ep'=8,'tp'=4] {'ep'}, dimensions={0}, use_global_device_ids=true | all-gather | bytes 294912 | tf_op jit(solution)/shard_map/all_gather | solution.py:223
  256.7 30.5 %all-reduce.7.cloned.1.call-done = bf16[128,256]{1,0:T(8,128)(2,1)} async-done(((bf16[128,256]{1,0:T(8,128)(2,1)}), bf16[128,256]{1,0:T(8,128)(2,1)}) %all-reduce.7.cloned.1.call-update) | async-done | bytes 65552 | tf_op jit(solution)/shard_map/psum | solution.py:227
  287.3 1.5 fusion.19
  (140 shorter events, 24.2 us)
Async XLA Ops:
  7.2 182.7 %copy-start = (bf16[2,256,2048]{2,1,0:T(8,128)(2,1)S(1)}, bf16[2,256,2048]{2,1,0:T(8,128)(2,1)}, u32[]{:S(2)}) copy-start(bf16[2,256,2048]{2,1,0:T(8,128)(2,1)} %param.45) | copy-start | bytes 6291460
  7.2 30.1 %copy-start.16 = (s32[128,2]{0,1:T(2,128)S(1)}, s32[128,2]{0,1:T(2,128)}, u32[]{:S(2)}) copy-start(s32[128,2]{0,1:T(2,128)} %param.41) | copy-start | bytes 3076
  7.2 30.1 %copy-start.4 = (f32[16,4,1024]{2,1,0:T(4,128)S(1)}, f32[16,4,1024]{2,1,0:T(4,128)}, u32[]{:S(2)}) copy-start(f32[16,4,1024]{2,1,0:T(4,128)} %param.36) | copy-start | bytes 786436
  7.2 70.8 %reduce-scatter.3.cloned.1.call-start = ((), (), s32[]{:S(2)}) async-start(), calls=%async_computation.4 | async-start | bytes 589824 | tf_op jit(solution)/shard_map/reduce_scatter | solution.py:81
  12.5 143.3 %all-reduce.5.cloned.1.call-start = ((), (), s32[]{:S(2)}) async-start(), calls=%async_computation.5 | async-start | bytes 262144 | tf_op jit(solution)/shard_map/psum | solution.py:149
  37.3 7.3 %copy-start.22 = (f32[16]{0:T(128)S(1)}, f32[16]{0:T(128)}, u32[]{:S(2)}) copy-start(f32[16]{0:T(128)} %param.28) | copy-start | bytes 196
  37.3 10.5 %copy-start.17 = (f32[128]{0:T(128)S(1)}, f32[128]{0:T(128)}, u32[]{:S(2)}) copy-start(f32[128]{0:T(128)} %param.33) | copy-start | bytes 1540
  37.4 42.7 %copy-start.18 = (f32[128]{0:T(128)S(1)}, f32[128]{0:T(128)}, u32[]{:S(2)}) copy-start(f32[128]{0:T(128)} %param.32) | copy-start | bytes 1540
  47.8 38.4 %copy-start.12 = (s32[16,3]{0,1:T(4,128)}, s32[16,3]{0,1:T(4,128)S(1)}, u32[]{:S(2)}) copy-start(s32[16,3]{0,1:T(4,128)S(1)} %reduce-window.9) | copy-start | bytes 580
  87.3 36.7 %copy-start.8 = (bf16[512,256]{1,0:T(8,128)(2,1)S(1)}, bf16[512,256]{1,0:T(8,128)(2,1)}, u32[]{:S(2)}) copy-start(bf16[512,256]{1,0:T(8,128)(2,1)} %param.38) | copy-start | bytes 786436
  87.3 37.6 %slice-start = ((s32[16,3]{0,1:T(4,128)}), s32[16,2]{0,1:T(2,128)S(1)}, s32[]{:S(2)}) async-start(s32[16,3]{0,1:T(4,128)} %copy-done.12), calls=%async_computation.8 | async-start | bytes 2048 | tf_op jit(solution)/shard_map/slice.1
  87.3 37.6 %copy-start.13 = (s32[256]{0:T(256)S(1)}, s32[256]{0:T(256)}, u32[]{:S(2)}) copy-start(s32[256]{0:T(256)} %reshape.203) | copy-start | bytes 3076
  87.3 69.5 %copy-start.5 = (bf16[256,1024]{1,0:T(8,128)(2,1)S(1)}, bf16[256,1024]{1,0:T(8,128)(2,1)}, u32[]{:S(2)}) copy-start(bf16[256,1024]{1,0:T(8,128)(2,1)} %param.48) | copy-start | bytes 1572868
  92.7 64.4 %copy-start.6 = (bf16[256,1024]{1,0:T(8,128)(2,1)S(1)}, bf16[256,1024]{1,0:T(8,128)(2,1)}, u32[]{:S(2)}) copy-start(bf16[256,1024]{1,0:T(8,128)(2,1)} %param.47) | copy-start | bytes 1572868
  124.9 99.1 %reduce-scatter.5.cloned.1.call-start = ((), (), s32[]{:S(2)}) async-start(), calls=%async_computation.6 | async-start | bytes 1179648 | tf_op jit(solution)/shard_map/reduce_scatter | solution.py:204
  156.8 8.1 %copy-start.2 = (bf16[128,256]{1,0:T(8,128)(2,1)}, bf16[128,256]{1,0:T(8,128)(2,1)S(1)}, u32[]{:S(2)}) copy-start(bf16[128,256]{1,0:T(8,128)(2,1)S(1)} %get-tuple-element.12) | copy-start | bytes 196612
  157.3 7.6 %copy-start.23 = (bf16[256,1]{0,1:T(2,128)(2,1)S(1)}, bf16[256,1]{0,1:T(2,128)(2,1)}, u32[]{:S(2)}) copy-start(bf16[256,1]{0,1:T(2,128)(2,1)} %reshape.229) | copy-start | bytes 1540
  159.4 28.3 %all-to-all-start = ((bf16[8,2,24,256]{3,2,1,0:T(8,128)(2,1)}), bf16[8,2,24,256]{3,2,1,0:T(8,128)(2,1)S(1)}, u32[]{:S(2)}, u32[]{:S(2)}) async-start(bf16[8,2,24,256]{3,2,1,0:T(8,128)(2,1)} %bitcast.9), calls=%async_computation.1 | async-start | bytes 393216 | tf_op jit(solution)/shard_map/all_to_all | solution.py:172
  195.0 11.1 %all-to-all-start.1 = ((bf16[8,2,6144]{2,1,0:T(2,128)(2,1)}), bf16[8,2,6144]{2,1,0:T(2,128)(2,1)S(1)}, u32[]{:S(2)}, u32[]{:S(2)}) async-start(bf16[8,2,6144]{2,1,0:T(2,128)(2,1)} %reshape.232), calls=%async_computation.2 | async-start | bytes 393216 | tf_op jit(solution)/shard_map/all_to_all | solution.py:194
  198.4 88.9 %all-reduce.7.cloned.1.call-start = ((), (), s32[]{:S(2)}) async-start(), calls=%async_computation.7 | async-start | bytes 131072 | tf_op jit(solution)/shard_map/psum | solution.py:227
  208.2 15.8 %copy-start.19 = (f32[16]{0:T(128)S(1)}, f32[16]{0:T(128)}, u32[]{:S(2)}) copy-start(f32[16]{0:T(128)} %dynamic_slice.35) | copy-start | bytes 196
  208.2 47.7 %copy-start.7 = (bf16[1024,256]{1,0:T(8,128)(2,1)S(1)}, bf16[1024,256]{1,0:T(8,128)(2,1)}, u32[]{:S(2)}) copy-start(bf16[1024,256]{1,0:T(8,128)(2,1)} %param.49) | copy-start | bytes 1572868
  208.2 47.7 %copy-start.14 = (f32[128]{0:T(128)S(1)}, f32[128]{0:T(128)}, u32[]{:S(2)}) copy-start(f32[128]{0:T(128)} %get-tuple-element.19) | copy-start | bytes 1540
  208.2 79.1 %copy-start.3 = (bf16[128,256]{1,0:T(8,128)(2,1)S(1)}, bf16[128,256]{1,0:T(8,128)(2,1)}, u32[]{:S(2)}) copy-start(bf16[128,256]{1,0:T(8,128)(2,1)} %copy-done.2) | copy-start | bytes 196612
  (7 other events, 37.2 us)
Sparse Core Ops, SparseCore 0:
  12.6 65.3 reduce-scatter.2
  125.0 30.7 all-reduce.4
  159.2 64.7 reduce-scatter.4
  256.8 30.3 all-reduce.6
where the time goes:
time: 296 us; the launch traced here: 295 us
  waiting for transfers between devices  110 us (37%)
  blocking collectives  107 us (36%)
  matrix products  23 us (8%)
  local copies, waits for them, and re-layouts  21 us (7%)
  between operations  14.4 us (5%)
  other arithmetic  10.8 us (4%)
  starting transfers between devices  9.25 us (3%)
    all_gather x1, blocking collectives, on_device(): lax.all_gather(dense_hidden, 'ep', axis=0, tiled=True)  30.9 us
    psum x1, waiting for transfers between devices, on_device(): attn_out = lax.psum(attn_part, 'tp')  30.6 us
    psum x1, waiting for transfers between devices, on_device(): lax.psum((routed + mix_share[:, None] * dense_part).astype(jnp.bfloat16),...  30.5 us
    all_gather x1, blocking collectives, on_device(): lax.all_gather(heads_out, 'ep', axis=0, tiled=True)  30.5 us
    reduce_scatter x1, waiting for transfers between devices, on_device(): lax.psum_scatter(jnp.concatenate([jnp.dot(selected, query_weight, preferr...  30.2 us
    psum x1, blocking collectives, on_device(): lax.psum((jnp.sum(stream * stream, axis=1), jnp.dot(normed_in, forget_row...  23.6 us
    psum x1, blocking collectives, on_device(): lax.psum((jnp.sum(middle * middle, axis=1), mix_part), 'ep')  21.9 us
    reduce_scatter x1, waiting for transfers between devices, on_device(): lax.psum_scatter(jnp.concatenate([jnp.dot(selected, dense_gate, preferred...  13.5 us
  transfers between devices with their start and end apart: 6, of which 5 were waited for; matrix products, arithmetic and copies ran while one was open for 9% of the time, Pallas kernels for 0%

commit v1 on v0

--- a/solution.py
+++ b/solution.py
@@ -146,7 +146,7 @@
         output_weight,
         preferred_element_type=jnp.float32,
     )
-    attn_out = lax.psum(attn_part, "tp")
+    attn_out = jnp.sum(lax.all_gather(attn_part, "tp"), axis=0)
     middle = (stream + attn_out).astype(jnp.bfloat16).astype(jnp.float32)
     normed_mid = (middle * lax.dynamic_slice_in_dim(ffn_gain, col_start, width_block)).astype(
         jnp.bfloat16

time: 296 us -> 269 us (0.909)
  waiting for transfers between devices: 110 us -> 79.8 us
  blocking collectives: 107 us -> 114 us
    psum x1 -> x0, waiting for transfers between devices: 30.6 us -> none  [on_device(): attn_out = lax.psum(attn_part, 'tp')]
    all_gather x0 -> x1, blocking collectives: none -> 7.13 us  [on_device(): attn_out = jnp.sum(lax.all_gather(attn_part, 'tp'), axis=0)]
    unnamed x54 -> x46, local copies, waits for them, and re-layouts: 9.15 us -> 9.7 us
  transfers between devices with their start and end apart: 6 -> 5, of which waited for: 5 -> 4; matrix products, arithmetic and copies ran while one was open for 9% -> 10% of each run, Pallas kernels for 0% -> 0%
where the time goes in v1:
time: 269 us; the launch traced here: 268 us
  blocking collectives  114 us (42%)
  waiting for transfers between devices  79.8 us (30%)
  matrix products  22.7 us (8%)
  local copies, waits for them, and re-layouts  19.6 us (7%)
  between operations  14.3 us (5%)
  other arithmetic  10 us (4%)
  starting transfers between devices  7.35 us (3%)
    all_gather x1, blocking collectives, on_device(): lax.all_gather(dense_hidden, 'ep', axis=0, tiled=True)  30.9 us
    reduce_scatter x1, waiting for transfers between devices, on_device(): lax.psum_scatter(jnp.concatenate([jnp.dot(selected, query_weight, preferr...  30.7 us
    all_gather x1, blocking collectives, on_device(): lax.all_gather(heads_out, 'ep', axis=0, tiled=True)  30.7 us
    psum x1, waiting for transfers between devices, on_device(): lax.psum((routed + mix_share[:, None] * dense_part).astype(jnp.bfloat16),...  30.6 us
    psum x1, blocking collectives, on_device(): lax.psum((jnp.sum(stream * stream, axis=1), jnp.dot(normed_in, forget_row...  23.9 us
    psum x1, blocking collectives, on_device(): lax.psum((jnp.sum(middle * middle, axis=1), mix_part), 'ep')  21.9 us
    reduce_scatter x1, waiting for transfers between devices, on_device(): lax.psum_scatter(jnp.concatenate([jnp.dot(selected, dense_gate, preferred...  13.4 us
    unnamed x46, local copies, waits for them, and re-layouts  9.7 us
  transfers between devices with their start and end apart: 5, of which 4 were waited for; matrix products, arithmetic and copies ran while one was open for 10% of the time, Pallas kernels for 0%

profile of v1, /device:TPU:0, one launch (start us, length us, event | category | flops | bytes accessed | tf_op | source)
XLA Modules:
  0.0 268.2 jit_solution(12008794366943263261)
XLA Ops:
  8.2 1.2 fusion.40
  10.5 1.1 fusion.38
  12.8 4.7 %copy.71 = f32[16,4,1024]{1,2,0:T(8,128)} copy(f32[16,4,1024]{2,1,0:T(4,128)S(1)} %copy-done.4) | data formatting | bytes 524288 | tf_op args[11]
  18.9 23.9 %all-reduce.1 = (f32[128,16]{0,1:T(8,128)S(1)}, f32[128]{0:T(128)S(1)}) all-reduce(f32[128,16]{0,1:T(8,128)S(1)} %fusion.34, f32[128]{0:T(128)S(1)} %fusion.15), channel_id=1, replica_groups=mesh['ep'=8,'tp'=4] {'ep'}, use_global_device_ids=true, to_apply=%region_2.0 | all-reduce | flops 2176 | bytes 17408 | tf_op jit(solution)/shard_map/psum | solution.py:70
  42.9 1.3 gather_fusion.1
  47.4 30.7 %reduce-scatter.3.cloned.1.call-done = f32[16,1024]{1,0:T(8,128)} async-done(((f32[128,1024]{1,0:T(8,128)}), f32[16,1024]{1,0:T(8,128)}) %reduce-scatter.3.cloned.1.call-update) | async-done | bytes 65552 | tf_op jit(solution)/shard_map/reduce_scatter | solution.py:81
  80.4 5.8 %fusion.64 = (f32[16,2,2]{2,1,0:T(2,128)S(1)}, f32[16,2,2,1024]{3,2,1,0:T(2,128)S(1)}) fusion(f32[16,2,2,1024]{3,2,1,0:T(2,128)S(1)} %reshape.201, f32[16,2,2]{2,1,0:T(2,128)S(1)} %copy.73, bf16[16,2,2,128]{3,2,1,0:T(2,128)(2,1)S(1)} %multiply_convert_fusion, bf16[16,2,1024,128]{3,2,1,0:T(8,128)(2,1)} %param.34, pred[16,1024]{1,0:T(8,128)(4,1)S(1)} %iota_compare_fusion.1), kind=kOutput, calls=%fused_computation.109 | convolution fusion | flops 17104832 | bytes 8946176 | tf_op jit(solution)/shard_map/skgd,skcd->skgc/dot_general | solution.py:116
  87.8 4.7 %fusion.9 = bf16[16,2,2,128]{3,2,1,0:T(2,128)(2,1)S(1)} fusion(bf16[16,2,1024,128]{3,2,1,0:T(8,128)(2,1)} %param.35, f32[16,2,2,1024]{3,2,1,0:T(2,128)S(1)} %get-tuple-element.22, f32[16,2,2]{2,1,0:T(2,128)S(1)} %multiply_maximum_fusion, f32[16,2,2]{2,1,0:T(2,128)S(1)} %get-tuple-element.13, f32[16,2,128]{2,1,0:T(2,128)S(1)} %reshape.207, ...), kind=kOutput, calls=%fused_computation.18 | convolution fusion | flops 16941056 | bytes 8684288 | tf_op jit(solution)/shard_map/skgc,skcd->skgd/dot_general | solution.py:132
  92.6 30.7 %all_gather.12 = bf16[128,512]{1,0:T(8,128)(2,1)S(1)} all-gather(bf16[16,512]{1,0:T(8,128)(2,1)S(1)} %convert_element_type.102), channel_id=1, replica_groups=mesh['ep'=8,'tp'=4] {'ep'}, dimensions={0}, use_global_device_ids=true | all-gather | bytes 147456 | tf_op jit(solution)/shard_map/all_gather | solution.py:145
  123.4 7.1 %all-gather = f32[512,256]{1,0:T(8,128)S(1)} all-gather(f32[128,256]{1,0:T(8,128)S(1)} %fusion.65), channel_id=2, replica_groups=mesh['ep'=8,'tp'=4] {'tp'}, dimensions={0}, use_global_device_ids=true | all-gather | bytes 655360 | tf_op jit(solution)/shard_map/all_gather | solution.py:149
  131.0 1.3 fusion.30
  134.3 3.7 %all-to-all-start = ((bf16[8,2,24,256]{3,2,1,0:T(8,128)(2,1)}), bf16[8,2,24,256]{3,2,1,0:T(8,128)(2,1)S(1)}, u32[]{:S(2)}, u32[]{:S(2)}) async-start(bf16[8,2,24,256]{3,2,1,0:T(8,128)(2,1)} %bitcast.10), calls=%async_computation.1 | async-start | bytes 393216 | tf_op jit(solution)/shard_map/all_to_all | solution.py:172
  138.1 21.9 %all-reduce = (f32[128]{0:T(128)S(1)}, f32[128]{0:T(128)S(1)}) all-reduce(f32[128]{0:T(128)S(1)} %get-tuple-element.11, f32[128]{0:T(128)S(1)} %convolution_bitcast_fusion), channel_id=1, replica_groups=mesh['ep'=8,'tp'=4] {'ep'}, use_global_device_ids=true, to_apply=%region_14.15 | all-reduce | flops 256 | bytes 2048 | tf_op jit(solution)/shard_map/psum | solution.py:159
  160.9 1.9 convolution_multiply_fusion.3
  162.9 2.3 fusion
  166.0 2.0 reshape.233
  168.0 3.4 %all-to-all-start.1 = ((bf16[8,2,6144]{2,1,0:T(2,128)(2,1)}), bf16[8,2,6144]{2,1,0:T(2,128)(2,1)S(1)}, u32[]{:S(2)}, u32[]{:S(2)}) async-start(bf16[8,2,6144]{2,1,0:T(2,128)(2,1)} %reshape.233), calls=%async_computation.2 | async-start | bytes 393216 | tf_op jit(solution)/shard_map/all_to_all | solution.py:194
  174.0 5.2 %all-to-all-done.1 = bf16[8,2,6144]{2,1,0:T(2,128)(2,1)S(1)} async-done(((bf16[8,2,6144]{2,1,0:T(2,128)(2,1)}), bf16[8,2,6144]{2,1,0:T(2,128)(2,1)S(1)}, u32[]{:S(2)}, u32[]{:S(2)}) %all-to-all-start.1) | async-done | bytes 196640 | tf_op jit(solution)/shard_map/all_to_all | solution.py:194
  179.2 1.5 reshape.234
  181.2 1.2 gather_fusion
  183.5 13.4 %reduce-scatter.5.cloned.1.call-done = f32[16,2048]{1,0:T(8,128)} async-done(((f32[128,2048]{1,0:T(8,128)}), f32[16,2048]{1,0:T(8,128)}) %reduce-scatter.5.cloned.1.call-update) | async-done | bytes 131088 | tf_op jit(solution)/shard_map/reduce_scatter | solution.py:204
  197.9 30.9 %all_gather.15 = bf16[128,1024]{1,0:T(8,128)(2,1)S(1)} all-gather(bf16[16,1024]{1,0:T(8,128)(2,1)S(1)} %fusion.22), channel_id=1, replica_groups=mesh['ep'=8,'tp'=4] {'ep'}, dimensions={0}, use_global_device_ids=true | all-gather | bytes 294912 | tf_op jit(solution)/shard_map/all_gather | solution.py:223
  229.6 30.6 %all-reduce.4.cloned.1.call-done = bf16[128,256]{1,0:T(8,128)(2,1)} async-done(((bf16[128,256]{1,0:T(8,128)(2,1)}), bf16[128,256]{1,0:T(8,128)(2,1)}) %all-reduce.4.cloned.1.call-update) | async-done | bytes 65552 | tf_op jit(solution)/shard_map/psum | solution.py:227
  260.2 1.5 fusion.19
  (130 shorter events, 22.2 us)
Async XLA Ops:
  7.2 155.7 %copy-start = (bf16[2,256,2048]{2,1,0:T(8,128)(2,1)S(1)}, bf16[2,256,2048]{2,1,0:T(8,128)(2,1)}, u32[]{:S(2)}) copy-start(bf16[2,256,2048]{2,1,0:T(8,128)(2,1)} %param.45) | copy-start | bytes 6291460
  7.2 5.4 %copy-start.1 = (bf16[128,256]{1,0:T(8,128)(2,1)S(1)}, bf16[128,256]{1,0:T(8,128)(2,1)}, u32[]{:S(2)}) copy-start(bf16[128,256]{1,0:T(8,128)(2,1)} %param.25) | copy-start | bytes 196612
  7.2 5.5 %copy-start.17 = (s32[16]{0:T(128)S(1)}, s32[16]{0:T(128)}, u32[]{:S(2)}) copy-start(s32[16]{0:T(128)} %param.37) | copy-start | bytes 196
  7.2 5.5 %copy-start.4 = (f32[16,4,1024]{2,1,0:T(4,128)S(1)}, f32[16,4,1024]{2,1,0:T(4,128)}, u32[]{:S(2)}) copy-start(f32[16,4,1024]{2,1,0:T(4,128)} %param.36) | copy-start | bytes 786436
  7.2 70.8 %reduce-scatter.3.cloned.1.call-start = ((), (), s32[]{:S(2)}) async-start(), calls=%async_computation.4 | async-start | bytes 589824 | tf_op jit(solution)/shard_map/reduce_scatter | solution.py:81
  12.5 184.4 %reduce-scatter.5.cloned.1.call-start = ((), (), s32[]{:S(2)}) async-start(), calls=%async_computation.5 | async-start | bytes 1179648 | tf_op jit(solution)/shard_map/reduce_scatter | solution.py:204
  12.7 4.9 %copy-start.18 = (s32[128]{0:T(128)S(1)}, s32[128]{0:T(128)}, u32[]{:S(2)}) copy-start(s32[128]{0:T(128)} %param.40) | copy-start | bytes 1540
  12.7 4.9 %copy-start.13 = (s32[128,2]{0,1:T(2,128)S(1)}, s32[128,2]{0,1:T(2,128)}, u32[]{:S(2)}) copy-start(s32[128,2]{0,1:T(2,128)} %param.41) | copy-start | bytes 3076
  12.7 31.6 %copy-start.19 = (f32[16]{0:T(128)S(1)}, f32[16]{0:T(128)}, u32[]{:S(2)}) copy-start(f32[16]{0:T(128)} %param.28) | copy-start | bytes 196
  12.8 34.5 %copy-start.14 = (f32[128]{0:T(128)S(1)}, f32[128]{0:T(128)}, u32[]{:S(2)}) copy-start(f32[128]{0:T(128)} %param.33) | copy-start | bytes 1540
  12.8 67.3 %copy-start.15 = (f32[128]{0:T(128)S(1)}, f32[128]{0:T(128)}, u32[]{:S(2)}) copy-start(f32[128]{0:T(128)} %param.32) | copy-start | bytes 1540
  80.3 6.3 %copy-start.9 = (f32[16,1024]{1,0:T(8,128)S(1)}, f32[16,1024]{1,0:T(8,128)}, u32[]{:S(2)}) copy-start(f32[16,1024]{1,0:T(8,128)} %reduce-scatter.3.cloned.1.call-done) | copy-start | bytes 196612
  87.8 35.4 %copy-start.7 = (bf16[512,256]{1,0:T(8,128)(2,1)S(1)}, bf16[512,256]{1,0:T(8,128)(2,1)}, u32[]{:S(2)}) copy-start(bf16[512,256]{1,0:T(8,128)(2,1)} %param.38) | copy-start | bytes 786436
  92.5 38.2 %copy-start.5 = (bf16[256,1024]{1,0:T(8,128)(2,1)S(1)}, bf16[256,1024]{1,0:T(8,128)(2,1)}, u32[]{:S(2)}) copy-start(bf16[256,1024]{1,0:T(8,128)(2,1)} %param.48) | copy-start | bytes 1572868
  130.7 7.2 %copy-start.2 = (bf16[128,256]{1,0:T(8,128)(2,1)}, bf16[128,256]{1,0:T(8,128)(2,1)S(1)}, u32[]{:S(2)}) copy-start(bf16[128,256]{1,0:T(8,128)(2,1)S(1)} %get-tuple-element.12) | copy-start | bytes 196612
  134.3 26.5 %all-to-all-start = ((bf16[8,2,24,256]{3,2,1,0:T(8,128)(2,1)}), bf16[8,2,24,256]{3,2,1,0:T(8,128)(2,1)S(1)}, u32[]{:S(2)}, u32[]{:S(2)}) async-start(bf16[8,2,24,256]{3,2,1,0:T(8,128)(2,1)} %bitcast.10), calls=%async_computation.1 | async-start | bytes 393216 | tf_op jit(solution)/shard_map/all_to_all | solution.py:172
  165.3 6.8 %copy-start.12 = (f32[128,2]{0,1:T(2,128)S(1)}, f32[128,2]{0,1:T(2,128)}, u32[]{:S(2)}) copy-start(f32[128,2]{0,1:T(2,128)} %param.42) | copy-start | bytes 3076
  168.0 11.1 %all-to-all-start.1 = ((bf16[8,2,6144]{2,1,0:T(2,128)(2,1)}), bf16[8,2,6144]{2,1,0:T(2,128)(2,1)S(1)}, u32[]{:S(2)}, u32[]{:S(2)}) async-start(bf16[8,2,6144]{2,1,0:T(2,128)(2,1)} %reshape.233), calls=%async_computation.2 | async-start | bytes 393216 | tf_op jit(solution)/shard_map/all_to_all | solution.py:194
  171.4 88.8 %all-reduce.4.cloned.1.call-start = ((), (), s32[]{:S(2)}) async-start(), calls=%async_computation.6 | async-start | bytes 131072 | tf_op jit(solution)/shard_map/psum | solution.py:227
  181.2 1.5 copy-start.8
  181.2 15.7 %copy-start.16 = (f32[16]{0:T(128)S(1)}, f32[16]{0:T(128)}, u32[]{:S(2)}) copy-start(f32[16]{0:T(128)} %dynamic_slice.35) | copy-start | bytes 196
  181.2 47.5 %copy-start.6 = (bf16[1024,256]{1,0:T(8,128)(2,1)S(1)}, bf16[1024,256]{1,0:T(8,128)(2,1)}, u32[]{:S(2)}) copy-start(bf16[1024,256]{1,0:T(8,128)(2,1)} %param.49) | copy-start | bytes 1572868
  181.2 47.5 %copy-start.11 = (f32[128]{0:T(128)S(1)}, f32[128]{0:T(128)}, u32[]{:S(2)}) copy-start(f32[128]{0:T(128)} %get-tuple-element.19) | copy-start | bytes 1540
  181.2 79.0 %copy-start.3 = (bf16[128,256]{1,0:T(8,128)(2,1)S(1)}, bf16[128,256]{1,0:T(8,128)(2,1)}, u32[]{:S(2)}) copy-start(bf16[128,256]{1,0:T(8,128)(2,1)} %copy-done.2) | copy-start | bytes 196612
  (1 other events, 0.6 us)
Sparse Core Ops, SparseCore 0:
  12.6 65.3 reduce-scatter.2
  133.5 63.3 reduce-scatter.4
  229.7 30.4 all-reduce.3
